TPU v7x, 128 devices: a whole 4x4x4 slice. The times are simulated.
128 devices in a mesh: sp: 16 (over z, x), tp: 8 (over y, core).
Axes of the slice: x: 4, y: 4, z: 4, core: 2. Of those that a mesh axis runs over, the one named last changes fastest.
Arguments:
- resid: bfloat16 [12288, 2048], P(('sp', 'tp')), may hold values from -6 to 6
- queries: bfloat16 [12288, 1024], P('sp', 'tp'), may hold values from -160 to 160
- keys: bfloat16 [12288, 1024], P('sp', 'tp'), may hold values from -6 to 6
- values: bfloat16 [12288, 1024], P('sp', 'tp'), may hold values from -6 to 6
- cum_gate: float32 [12288, 16], P('sp', 'tp'), may hold values from -1385 to 0, as said below
- out_weight: bfloat16 [1024, 2048], P('tp'), may hold values from -0.375 to 0.375
- norm_gain: float32 [2048], replicated, may hold values from 0.1 to 1.9
- gate_weight: bfloat16 [2048, 5504], P('sp', 'tp'), may hold values from -0.125 to 0.125
- up_weight: bfloat16 [2048, 5504], P('sp', 'tp'), may hold values from -0.125 to 0.125
- down_weight: bfloat16 [5504, 2048], P('tp', 'sp'), may hold values from -0.078125 to 0.078125
Outputs:
- layer_out: bfloat16 [12288, 2048], P(('sp', 'tp'))
Inputs may be any that keep to these rules, and one draw needn't show every extreme that they name: `cum_gate`: each column is non-increasing along positions and starts at or below zero.
All inputs are finite; a program needn't handle non-finite values.
Results may differ from a plain program's by a relative error of at most 0.01.
Values may be sent and summed in bfloat16 or wider, within the bound.
A program may use at most 256 MiB of HBM per device.

v0:
```python
import jax
import jax.numpy as jnp
from jax import lax
from jax.sharding import Mesh
from jax.sharding import PartitionSpec as P

HEAD_DIM = 64
TP = ("tp_0", "tp_1")
SP_TP = ("sp", "tp_0", "tp_1")


def turned_gather(arrays, axis, dims):
    turned = [jnp.moveaxis(a, dim, 0) for a, dim in zip(arrays, dims)]
    widths = [t[0].size for t in turned]
    both = jnp.concatenate([t.reshape(-1, w) for t, w in zip(turned, widths)], axis=1)
    out = lax.all_gather(both, axis, axis=0, tiled=True)
    blocks = jnp.split(out, [sum(widths[:k]) for k in range(1, len(widths))], axis=1)
    return tuple(
        (
            jnp.moveaxis(b.reshape(-1, *t.shape[1:]), 0, dim)
            for b, t, dim in zip(blocks, turned, dims)
        )
    )


def joined_along(blocks, dim):
    blocks = jnp.moveaxis(blocks, 0, dim)
    lengths = blocks.shape
    return blocks.reshape(*lengths[:dim], lengths[dim] * lengths[dim + 1], *lengths[dim + 2 :])


def copy_for_each(value, axis):
    count = lax.axis_size(axis)
    return lax.all_to_all(
        jnp.broadcast_to(value[None], (count, *value.shape)), axis, 0, 0, tiled=True
    )


def gathered_copies(value, axis, dim):
    return joined_along(copy_for_each(value, axis), dim)


def sent_together(arrays, axis, dim, along):
    ends, at = ([], 0)
    for a in arrays[:-1]:
        at += a.shape[along]
        ends.append(at)
    both = jnp.concatenate(arrays, axis=along)
    return tuple(jnp.split(lax.all_gather(both, axis, axis=dim, tiled=True), ends, axis=along))


def sum_by_axis(value, axes, dim):
    for axis in axes:
        value = lax.psum_scatter(value, axis, scatter_dimension=dim, tiled=True)
    return value


def rms_norm(mixed, norm_gain):
    scaled = mixed * lax.rsqrt(jnp.mean(mixed * mixed, axis=-1, keepdims=True) + 1e-06) * norm_gain
    return scaled.astype(jnp.bfloat16)


def rounded(term):
    return term.astype(jnp.bfloat16).astype(jnp.float32)


def local(
    resid,
    queries,
    keys,
    values,
    cum_gate,
    out_weight,
    norm_gain,
    gate_weight,
    up_weight,
    down_weight,
):
    rows = queries.shape[0]
    heads_here = cum_gate.shape[1]
    scale = HEAD_DIM ** (-0.5)
    whole_gate, whole_up, whole_down = turned_gather(
        (gate_weight, up_weight, down_weight), "sp", (0, 0, 1)
    )
    proj_weight = lax.all_gather(out_weight, TP, axis=0, tiled=True)
    first = lax.axis_index("sp") * rows
    gates_all = gathered_copies(cum_gate, "sp", 0)
    query_heads = queries.reshape(rows, heads_here, HEAD_DIM)
    query_pos = first + jnp.arange(rows, dtype=jnp.int32)
    query_gate = cum_gate.T
    best = jnp.full((heads_here, rows), -1e30, jnp.float32)
    key_piece, value_piece = sent_together((keys, values), "sp", 0, 1)
    count = key_piece.shape[0]
    key_heads = key_piece.reshape(count, heads_here, HEAD_DIM)
    value_heads = value_piece.reshape(count, heads_here, HEAD_DIM)
    key_gate = gates_all.T
    score = (
        jnp.einsum("qhd,khd->hqk", query_heads, key_heads, preferred_element_type=jnp.float32)
        * scale
    )
    score = score + query_gate[:, :, None] - key_gate[:, None, :]
    key_pos = jnp.arange(count, dtype=jnp.int32)
    score = jnp.where(key_pos[None, None, :] <= query_pos[None, :, None], score, -jnp.inf)
    new_best = jnp.maximum(best, jnp.max(score, axis=-1))
    weight = jnp.exp(score - new_best[:, :, None])
    total = jnp.sum(weight, axis=-1)
    numer = jnp.einsum(
        "hqk,khd->hqd", weight.astype(jnp.bfloat16), value_heads, preferred_element_type=jnp.float32
    )
    best, total, numer = (new_best, total, numer)
    attn = (
        (numer / total[:, :, None])
        .transpose(1, 0, 2)
        .reshape(rows, heads_here * HEAD_DIM)
        .astype(jnp.bfloat16)
    )
    groups = lax.axis_size(TP)
    share = rows // groups
    own_rows = lax.all_to_all(attn, TP, split_axis=0, concat_axis=1, tiled=True)
    group_width = attn.shape[1]
    row_groups = own_rows.reshape(share, groups, group_width)
    weight_groups = proj_weight.reshape(groups, group_width, proj_weight.shape[1])
    terms = jnp.einsum(
        "rgc,gcd->grd", row_groups, weight_groups, preferred_element_type=jnp.float32
    )
    proj = jnp.sum(rounded(terms), axis=0)
    mixed = resid.astype(jnp.float32) + proj
    normed_all = lax.all_gather(rms_norm(mixed, norm_gain), TP, axis=0, tiled=True)
    gate = jnp.dot(normed_all, whole_gate, preferred_element_type=jnp.float32)
    upper = jnp.dot(normed_all, whole_up, preferred_element_type=jnp.float32)
    hidden = (jax.nn.silu(gate) * upper).astype(jnp.bfloat16)
    ffn_part = jnp.dot(hidden, whole_down, preferred_element_type=jnp.float32)
    ffn = sum_by_axis(rounded(ffn_part).astype(jnp.bfloat16), TP, 0).astype(jnp.float32)
    return (mixed + 0.5 * ffn).astype(jnp.bfloat16)


def solution(mesh):
    split = Mesh(mesh.devices.reshape(mesh.shape["sp"], 4, 2), ("sp", "tp_0", "tp_1"))
    return jax.shard_map(
        local,
        mesh=split,
        in_specs=(
            P(SP_TP, None),
            P("sp", TP),
            P("sp", TP),
            P("sp", TP),
            P("sp", TP),
            P(TP, None),
            P(),
            P("sp", TP),
            P("sp", TP),
            P(TP, "sp"),
        ),
        out_specs=P(SP_TP, None),
        check_vma=False,
    )
```

profile of v0, /device:TPU:1, one launch (start us, length us, event | category | flops | bytes accessed | tf_op | source)
XLA Modules:
  0.0 297.3 jit_solution(10596566933157385455)
XLA Ops:
  6.5 0.0 all-gather.5.cloned.1.call-start
  6.5 1.8 pad_maximum_fusion.1
  8.3 0.0 copy-start.2
  8.3 0.0 all-gather.5.cloned.1.call-update
  8.4 0.0 all-gather.7.cloned.1.call-start
  8.4 0.7 all-gather.7.cloned.1.call-update
  9.1 1.4 broadcast_in_dim.17
  10.5 8.4 %all-to-all-start = ((f32[16,768,2]{1,2,0:T(2,128)}), f32[16,768,2]{1,2,0:T(2,128)S(1)}, u32[]{:S(2)}, u32[]{:S(2)}) async-start(f32[16,768,2]{1,2,0:T(2,128)} %broadcast_in_dim.17), calls=%async_computation | async-start | bytes 196608 | tf_op jit(solution)/shard_map/all_to_all | solution.py:34
  18.9 0.0 all-gather.11.cloned.1.call-start
  19.0 1.9 pad_maximum_fusion
  20.9 0.0 all-gather.11.cloned.1.call-update
  20.9 7.4 %iota_compare_fusion = pred[768,12288]{0,1:T(8,128)(4,1)} fusion(s32[768]{0:T(1024)S(1)} %iota_add_fusion), kind=kLoop, calls=%fused_computation.5 | loop fusion | flops 9437184 | bytes 9440256 | tf_op jit(solution)/shard_map/le | solution.py:103
  28.3 0.0 copy-done.2
  28.3 0.1 copy.22
  28.4 45.5 %all-gather.5.cloned.1.call-done = bf16[12288,256]{1,0:T(8,128)(2,1)} async-done(((bf16[768,256]{1,0:T(8,128)(2,1)}), bf16[12288,256]{1,0:T(8,128)(2,1)}) %all-gather.5.cloned.1.call-update) | async-done | bytes 6291472 | tf_op jit(solution)/shard_map/all_gather | solution.py:49
  73.9 4.3 %fusion.29 = (bf16[12288,128]{1,0:T(8,128)(2,1)}, bf16[12288,128]{1,0:T(8,128)(2,1)S(1)}) fusion(bf16[12288,256]{1,0:T(8,128)(2,1)} %all-gather.5.cloned.1.call-done), kind=kLoop, calls=%fused_computation.34 | loop fusion | bytes 12582912 | tf_op jit(solution)/shard_map/split | solution.py:49
  78.2 4.7 %copy.21 = bf16[12288,128]{0,1:T(8,128)(2,1)} copy(bf16[12288,128]{1,0:T(8,128)(2,1)} %get-tuple-element.5) | data formatting | bytes 6291456 | tf_op jit(solution)/shard_map/split | solution.py:49
  82.9 0.0 all-to-all-done
  83.0 0.0 copy-done.3
  83.0 33.3 %fusion.2 = (f32[2,768]{1,0:T(2,128)S(1)}, f32[2,12288,768]{2,1,0:T(8,128)}) fusion(f32[2,12288]{1,0:T(2,128)S(1)} %bitcast.45, f32[2,768]{1,0:T(2,128)S(1)} %bitcast.50, pred[768,12288]{0,1:T(8,128)(4,1)} %iota_compare_fusion, bf16[12288,2,64]{0,2,1:T(8,128)(2,1)} %bitcast.43, bf16[768,2,64]{0,2,1:T(8,128)(2,1)S(1)} %bitcast.48), kind=kOutput, calls=%fused_computation.4 | convolution fusion | flops 2510289408 | bytes 88387584 | tf_op jit(solution)/shard_map/qhd,khd->hqk/dot_general | solution.py:98
  116.2 2.8 copy.23
  119.1 27.7 %fusion = f32[2,768]{1,0:T(2,128)S(1)} fusion(f32[2,12288,768]{2,1,0:T(8,128)} %get-tuple-element.8, f32[2,768]{1,0:T(2,128)S(1)} %broadcast_maximum_fusion, f32[2,12288]{1,0:T(2,128)S(1)} %bitcast.46, f32[2,768]{1,0:T(2,128)S(1)} %bitcast.51, pred[768,12288]{0,1:T(8,128)(4,1)} %iota_compare_fusion), kind=kLoop, calls=%fused_computation.2 | loop fusion | flops 113244672 | bytes 85051392 | tf_op jit(solution)/shard_map/reduce_sum | solution.py:106
  146.8 0.0 copy-done.1
  146.8 30.7 %fusion.22 = bf16[768,2,64]{0,2,1:T(8,128)(2,1)S(1)} fusion(bf16[12288,2,64]{0,2,1:T(8,128)(2,1)S(1)} %bitcast.44, f32[2,12288,768]{2,1,0:T(8,128)} %get-tuple-element.8, f32[2,768]{1,0:T(2,128)S(1)} %broadcast_maximum_fusion, f32[2,12288]{1,0:T(2,128)S(1)} %bitcast.47, f32[2,768]{1,0:T(2,128)S(1)} %bitcast.52, pred[768,12288]{0,1:T(8,128)(4,1)} %iota_compare_fusion, ...), kind=kOutput, calls=%fused_computation.20 | convolution fusion | flops 2529361920 | bytes 88393728 | tf_op jit(solution)/shard_map/hqk,khd->hqd/dot_general | solution.py:107
  177.5 0.0 copy-start
  177.5 0.0 copy-start.4
  177.5 0.3 convert_element_type.39
  177.8 0.9 copy.25
  178.7 5.0 %all-to-all-start.1 = ((bf16[8,96,128]{2,1,0:T(8,128)(2,1)}), bf16[8,96,128]{2,1,0:T(8,128)(2,1)S(1)}, u32[]{:S(2)}, u32[]{:S(2)}) async-start(bf16[8,96,128]{2,1,0:T(8,128)(2,1)} %copy.25), calls=%async_computation.1 | async-start | bytes 393216 | tf_op jit(solution)/shard_map/all_to_all | solution.py:119
  183.7 0.0 all-gather.9.cloned.1.call-start
  183.8 5.9 %all-to-all-done.1 = bf16[8,96,128]{2,1,0:T(8,128)(2,1)S(1)} async-done(((bf16[8,96,128]{2,1,0:T(8,128)(2,1)}), bf16[8,96,128]{2,1,0:T(8,128)(2,1)S(1)}, u32[]{:S(2)}, u32[]{:S(2)}) %all-to-all-start.1) | async-done | bytes 196640 | tf_op jit(solution)/shard_map/all_to_all | solution.py:119
  189.6 3.2 %convert_reduce_fusion = f32[96,2048]{1,0:T(8,128)S(1)} fusion(bf16[8,128,2048]{2,1,0:T(8,128)(2,1)} %bitcast.42, bf16[8,96,128]{2,1,0:T(8,128)(2,1)S(1)} %all-to-all-done.1), kind=kOutput, calls=%fused_computation.8 | convolution fusion | flops 407175168 | bytes 5177344 | tf_op jit(solution)/shard_map/rgc,gcd->grd/dot_general | solution.py:123
  192.8 0.0 copy-done
  192.8 0.2 multiply_reduce_fusion
  193.0 0.0 copy-done.4
  193.0 0.9 multiply_convert_fusion.1
  193.9 0.0 all-gather.9.cloned.1.call-update
  193.9 0.2 reduce-scatter.3.cloned.1.call-start
  194.2 0.0 all-gather.11.cloned.1.call-done
  194.2 26.3 %all-gather.9.cloned.1.call-done = bf16[768,2048]{1,0:T(8,128)(2,1)} async-done(((bf16[96,2048]{1,0:T(8,128)(2,1)}), bf16[768,2048]{1,0:T(8,128)(2,1)}) %all-gather.9.cloned.1.call-update) | async-done | bytes 3145744 | tf_op jit(solution)/shard_map/all_gather | solution.py:128
  220.5 5.1 %fusion.9 = f32[768,688]{0,1:T(8,128)S(1)} fusion(bf16[768,2048]{1,0:T(8,128)(2,1)} %all-gather.9.cloned.1.call-done, bf16[2048,2064]{0,1:T(8,128)(2,1)} %all-gather.11.cloned.1.call-done), kind=kOutput, calls=%fused_computation.14 | convolution fusion | flops 2164260864 | bytes 8077312 | tf_op jit(solution)/shard_map/dot_general | solution.py:129
  225.6 11.7 %convolution_convert_fusion = bf16[768,2048]{1,0:T(8,128)(2,1)} fusion(bf16[2048,2064]{0,1:T(8,128)(2,1)} %all-gather.11.cloned.1.call-done, f32[768,688]{0,1:T(8,128)S(1)} %fusion.9, bf16[768,2048]{1,0:T(8,128)(2,1)} %all-gather.9.cloned.1.call-done), kind=kOutput, calls=%fused_computation.9 | convolution fusion | flops 4333264896 | bytes 14041088 | tf_op jit(solution)/shard_map/dot_general | solution.py:132
  237.3 0.0 reduce-scatter.3.cloned.1.call-update
  237.3 0.0 reduce-scatter.5.cloned.1.call-start
  237.4 37.9 %reduce-scatter.3.cloned.1.call-done = bf16[192,2048]{1,0:T(8,128)(2,1)} async-done(((bf16[768,2048]{1,0:T(8,128)(2,1)}), bf16[192,2048]{1,0:T(8,128)(2,1)}) %reduce-scatter.3.cloned.1.call-update) | async-done | bytes 786448 | tf_op jit(solution)/shard_map/reduce_scatter | solution.py:54
  275.2 0.0 reduce-scatter.5.cloned.1.call-update
  275.3 13.3 %reduce-scatter.5.cloned.1.call-done = bf16[96,2048]{1,0:T(8,128)(2,1)} async-done(((bf16[192,2048]{1,0:T(8,128)(2,1)}), bf16[96,2048]{1,0:T(8,128)(2,1)}) %reduce-scatter.5.cloned.1.call-update) | async-done | bytes 393232 | tf_op jit(solution)/shard_map/reduce_scatter | solution.py:54
  288.6 1.9 add_convert_fusion
  (6 shorter events, 0.0 us)
Async XLA Ops:
  6.5 67.4 %all-gather.5.cloned.1.call-start = ((), (), s32[]{:S(2)}) async-start(), calls=%async_computation.4 | async-start | bytes 6684672 | tf_op jit(solution)/shard_map/all_gather | solution.py:49
  8.3 19.9 %copy-start.2 = (bf16[768,128]{1,0:T(8,128)(2,1)S(1)}, bf16[768,128]{1,0:T(8,128)(2,1)}, u32[]{:S(2)}) copy-start(bf16[768,128]{1,0:T(8,128)(2,1)} %param.11) | copy-start | bytes 589828
  8.4 175.4 %all-gather.7.cloned.1.call-start = ((), (), s32[]{:S(2)}) async-start(), calls=%async_computation.5 | async-start | bytes 4718592 | tf_op jit(solution)/shard_map/all_gather | solution.py:85
  10.5 72.5 %all-to-all-start = ((f32[16,768,2]{1,2,0:T(2,128)}), f32[16,768,2]{1,2,0:T(2,128)S(1)}, u32[]{:S(2)}, u32[]{:S(2)}) async-start(f32[16,768,2]{1,2,0:T(2,128)} %broadcast_in_dim.17), calls=%async_computation | async-start | bytes 196608 | tf_op jit(solution)/shard_map/all_to_all | solution.py:34
  18.9 175.3 %all-gather.11.cloned.1.call-start = ((), (), s32[]{:S(2)}) async-start(), calls=%async_computation.7 | async-start | bytes 8982528 | tf_op jit(solution)/shard_map/all_gather | solution.py:16
  78.2 4.7 %copy-start.3 = (f32[768,2]{0,1:T(2,128)S(1)}, f32[768,2]{0,1:T(2,128)}, u32[]{:S(2)}) copy-start(f32[768,2]{0,1:T(2,128)} %param.14) | copy-start | bytes 18436
  119.1 27.8 %copy-start.1 = (bf16[12288,128]{0,1:T(8,128)(2,1)S(1)}, bf16[12288,128]{0,1:T(8,128)(2,1)}, u32[]{:S(2)}) copy-start(bf16[12288,128]{0,1:T(8,128)(2,1)} %copy.23) | copy-start | bytes 9437188
  177.5 15.3 %copy-start = (bf16[96,2048]{1,0:T(8,128)(2,1)S(1)}, bf16[96,2048]{1,0:T(8,128)(2,1)}, u32[]{:S(2)}) copy-start(bf16[96,2048]{1,0:T(8,128)(2,1)} %param.10) | copy-start | bytes 1179652
  177.5 15.5 %copy-start.4 = (f32[2048]{0:T(1024)S(1)}, f32[2048]{0:T(1024)}, u32[]{:S(2)}) copy-start(f32[2048]{0:T(1024)} %param.16) | copy-start | bytes 24580
  178.7 10.9 %all-to-all-start.1 = ((bf16[8,96,128]{2,1,0:T(8,128)(2,1)}), bf16[8,96,128]{2,1,0:T(8,128)(2,1)S(1)}, u32[]{:S(2)}, u32[]{:S(2)}) async-start(bf16[8,96,128]{2,1,0:T(8,128)(2,1)} %copy.25), calls=%async_computation.1 | async-start | bytes 393216 | tf_op jit(solution)/shard_map/all_to_all | solution.py:119
  183.7 36.7 %all-gather.9.cloned.1.call-start = ((), (), s32[]{:S(2)}) async-start(), calls=%async_computation.6 | async-start | bytes 3538944 | tf_op jit(solution)/shard_map/all_gather | solution.py:128
  193.9 81.3 %reduce-scatter.3.cloned.1.call-start = ((), (), s32[]{:S(2)}) async-start(), calls=%async_computation.8 | async-start | bytes 3932160 | tf_op jit(solution)/shard_map/reduce_scatter | solution.py:54
  237.3 51.2 %reduce-scatter.5.cloned.1.call-start = ((), (), s32[]{:S(2)}) async-start(), calls=%async_computation.9 | async-start | bytes 1179648 | tf_op jit(solution)/shard_map/reduce_scatter | solution.py:54
Sparse Core Ops, SparseCore 0:
  9.5 64.4 all-gather.4
  75.7 32.1 all-gather.6
  110.0 75.8 all-gather.10
  194.1 26.3 all-gather.8
  237.5 37.7 reduce-scatter.2
  277.4 11.0 reduce-scatter.4
where the time goes:
time: 298 us; the launch traced here: 297 us
  waiting for transfers between devices  130 us (44%)
  matrix products  83.9 us (28%)
  other arithmetic  41.8 us (14%)
  local copies, waits for them, and re-layouts  14.5 us (5%)
  starting transfers between devices  13.8 us (5%)
  between operations  13.6 us (5%)
    reduce_scatter x2, waiting for transfers between devices, sum_by_axis(): value = lax.psum_scatter(value, axis, scatter_dimension=dim, tiled=True)  51.1 us
    all_gather x1, waiting for transfers between devices, sent_together(): lax.all_gather(both, axis, axis=dim, tiled=True)  45.5 us
    dot_general x1, matrix products, local(): jnp.einsum('qhd,khd->hqk', query_heads, key_heads, preferred_element_type...  33.3 us
    dot_general x1, matrix products, local(): jnp.einsum('hqk,khd->hqd', weight.astype(jnp.bfloat16), value_heads, pref...  30.7 us
    reduce_sum x1, other arithmetic, local(): total = jnp.sum(weight, axis=-1)  27.7 us
    all_gather x1, waiting for transfers between devices, local(): lax.all_gather(rms_norm(mixed, norm_gain), TP, axis=0, tiled=True)  26.3 us
    split x3, local copies, waits for them, and re-layouts, sent_together(): jnp.split(lax.all_gather(both, axis, axis=dim, tiled=True), ends, axis=al...  11.8 us
    dot_general x1, matrix products, local(): ffn_part = jnp.dot(hidden, whole_down, preferred_element_type=jnp.float32)  11.7 us
  transfers between devices with their start and end apart: 8, of which 5 were waited for; matrix products, arithmetic and copies ran while one was open for 40% of the time, Pallas kernels for 0%

commit v1 on v0

--- a/solution.py
+++ b/solution.py
@@ -125,7 +125,10 @@
     )
     proj = jnp.sum(rounded(terms), axis=0)
     mixed = resid.astype(jnp.float32) + proj
-    normed_all = lax.all_gather(rms_norm(mixed, norm_gain), TP, axis=0, tiled=True)
+    normed_all = jnp.concatenate(
+        lax.all_to_all(jnp.stack([rms_norm(mixed, norm_gain)] * lax.axis_size(TP)), TP, 0, 0),
+        axis=0,
+    )
     gate = jnp.dot(normed_all, whole_gate, preferred_element_type=jnp.float32)
     upper = jnp.dot(normed_all, whole_up, preferred_element_type=jnp.float32)
     hidden = (jax.nn.silu(gate) * upper).astype(jnp.bfloat16)

time: 298 us -> 311 us (1.044)
  blocking collectives: 0 us -> 41.6 us
  waiting for transfers between devices: 130 us -> 102 us
    all_to_all x0 -> x1, blocking collectives: none -> 41.6 us  [local(): lax.all_to_all(jnp.stack([rms_norm(mixed, norm_gain)] * lax.axis_size(TP)...]
    all_gather x1 -> x0, waiting for transfers between devices: 26.3 us -> none  [local(): lax.all_gather(rms_norm(mixed, norm_gain), TP, axis=0, tiled=True)]
  transfers between devices with their start and end apart: 8 -> 7, of which waited for: 5 -> 4; matrix products, arithmetic and copies ran while one was open for 40% -> 38% of each run, Pallas kernels for 0% -> 0%
where the time goes in v1:
time: 311 us; the launch traced here: 310 us
  waiting for transfers between devices  102 us (33%)
  matrix products  84 us (27%)
  blocking collectives  41.6 us (13%)
  other arithmetic  41.1 us (13%)
  local copies, waits for them, and re-layouts  14.9 us (5%)
  starting transfers between devices  13.6 us (4%)
  between operations  13.3 us (4%)
    reduce_scatter x2, waiting for transfers between devices, sum_by_axis(): value = lax.psum_scatter(value, axis, scatter_dimension=dim, tiled=True)  50 us
    all_gather x1, waiting for transfers between devices, sent_together(): lax.all_gather(both, axis, axis=dim, tiled=True)  45.5 us
    all_to_all x1, blocking collectives, local(): lax.all_to_all(jnp.stack([rms_norm(mixed, norm_gain)] * lax.axis_size(TP)...  41.6 us
    dot_general x1, matrix products, local(): jnp.einsum('qhd,khd->hqk', query_heads, key_heads, preferred_element_type...  33.3 us
    dot_general x1, matrix products, local(): jnp.einsum('hqk,khd->hqd', weight.astype(jnp.bfloat16), value_heads, pref...  30.7 us
    reduce_sum x1, other arithmetic, local(): total = jnp.sum(weight, axis=-1)  27.8 us
    split x3, local copies, waits for them, and re-layouts, sent_together(): jnp.split(lax.all_gather(both, axis, axis=dim, tiled=True), ends, axis=al...  11.8 us
    dot_general x1, matrix products, local(): ffn_part = jnp.dot(hidden, whole_down, preferred_element_type=jnp.float32)  11.7 us
  transfers between devices with their start and end apart: 7, of which 4 were waited for; matrix products, arithmetic and copies ran while one was open for 38% of the time, Pallas kernels for 0%

profile of v1, /device:TPU:1, one launch (start us, length us, event | category | flops | bytes accessed | tf_op | source)
XLA Modules:
  0.0 310.4 jit_solution(7463301329667845432)
XLA Ops:
  6.5 0.0 all-gather.4.cloned.1.call-start
  6.5 1.8 pad_maximum_fusion.1
  8.3 0.0 copy-start.2
  8.3 0.0 all-gather.4.cloned.1.call-update
  8.4 0.0 all-gather.6.cloned.1.call-start
  8.4 0.7 all-gather.6.cloned.1.call-update
  9.1 1.4 broadcast_in_dim.17
  10.5 8.4 %all-to-all-start = ((f32[16,768,2]{1,2,0:T(2,128)}), f32[16,768,2]{1,2,0:T(2,128)S(1)}, u32[]{:S(2)}, u32[]{:S(2)}) async-start(f32[16,768,2]{1,2,0:T(2,128)} %broadcast_in_dim.17), calls=%async_computation | async-start | bytes 196608 | tf_op jit(solution)/shard_map/all_to_all | solution.py:34
  18.9 0.0 all-gather.8.cloned.1.call-start
  19.0 1.9 pad_maximum_fusion
  20.9 0.0 all-gather.8.cloned.1.call-update
  20.9 7.4 %iota_compare_fusion = pred[768,12288]{0,1:T(8,128)(4,1)} fusion(s32[768]{0:T(1024)S(1)} %iota_add_fusion), kind=kLoop, calls=%fused_computation.5 | loop fusion | flops 9437184 | bytes 9440256 | tf_op jit(solution)/shard_map/le | solution.py:103
  28.3 0.0 copy-done.2
  28.3 0.1 copy.22
  28.5 45.5 %all-gather.4.cloned.1.call-done = bf16[12288,256]{1,0:T(8,128)(2,1)} async-done(((bf16[768,256]{1,0:T(8,128)(2,1)}), bf16[12288,256]{1,0:T(8,128)(2,1)}) %all-gather.4.cloned.1.call-update) | async-done | bytes 6291472 | tf_op jit(solution)/shard_map/all_gather | solution.py:49
  73.9 4.3 %fusion.29 = (bf16[12288,128]{1,0:T(8,128)(2,1)}, bf16[12288,128]{1,0:T(8,128)(2,1)S(1)}) fusion(bf16[12288,256]{1,0:T(8,128)(2,1)} %all-gather.4.cloned.1.call-done), kind=kLoop, calls=%fused_computation.34 | loop fusion | bytes 12582912 | tf_op jit(solution)/shard_map/split | solution.py:49
  78.2 0.0 copy-start.3
  78.2 4.7 %copy.21 = bf16[12288,128]{0,1:T(8,128)(2,1)} copy(bf16[12288,128]{1,0:T(8,128)(2,1)} %get-tuple-element.5) | data formatting | bytes 6291456 | tf_op jit(solution)/shard_map/split | solution.py:49
  82.9 0.0 all-to-all-done
  82.9 0.0 copy-done.3
  82.9 33.3 %fusion.2 = (f32[2,768]{1,0:T(2,128)S(1)}, f32[2,12288,768]{2,1,0:T(8,128)}) fusion(f32[2,12288]{1,0:T(2,128)S(1)} %bitcast.48, f32[2,768]{1,0:T(2,128)S(1)} %bitcast.53, pred[768,12288]{0,1:T(8,128)(4,1)} %iota_compare_fusion, bf16[12288,2,64]{0,2,1:T(8,128)(2,1)} %bitcast.44, bf16[768,2,64]{0,2,1:T(8,128)(2,1)S(1)} %bitcast.51), kind=kOutput, calls=%fused_computation.4 | convolution fusion | flops 2510289408 | bytes 88387584 | tf_op jit(solution)/shard_map/qhd,khd->hqk/dot_general | solution.py:98
  116.2 2.8 copy.23
  119.0 0.0 copy-start.1
  119.0 27.8 %fusion = f32[2,768]{1,0:T(2,128)S(1)} fusion(f32[2,12288,768]{2,1,0:T(8,128)} %get-tuple-element.8, f32[2,768]{1,0:T(2,128)S(1)} %broadcast_maximum_fusion, f32[2,12288]{1,0:T(2,128)S(1)} %bitcast.49, f32[2,768]{1,0:T(2,128)S(1)} %bitcast.54, pred[768,12288]{0,1:T(8,128)(4,1)} %iota_compare_fusion), kind=kLoop, calls=%fused_computation.2 | loop fusion | flops 113244672 | bytes 85051392 | tf_op jit(solution)/shard_map/reduce_sum | solution.py:106
  146.8 0.0 copy-done.1
  146.8 30.7 %fusion.22 = bf16[768,2,64]{0,2,1:T(8,128)(2,1)S(1)} fusion(bf16[12288,2,64]{0,2,1:T(8,128)(2,1)S(1)} %bitcast.45, f32[2,12288,768]{2,1,0:T(8,128)} %get-tuple-element.8, f32[2,768]{1,0:T(2,128)S(1)} %broadcast_maximum_fusion, f32[2,12288]{1,0:T(2,128)S(1)} %bitcast.50, f32[2,768]{1,0:T(2,128)S(1)} %bitcast.55, pred[768,12288]{0,1:T(8,128)(4,1)} %iota_compare_fusion, ...), kind=kOutput, calls=%fused_computation.20 | convolution fusion | flops 2529361920 | bytes 88393728 | tf_op jit(solution)/shard_map/hqk,khd->hqd/dot_general | solution.py:107
  177.5 0.0 copy-start
  177.5 0.0 copy-start.4
  177.5 0.3 convert_element_type.39
  177.8 0.9 copy.25
  178.7 5.1 %all-to-all-start.1 = ((bf16[8,96,128]{2,1,0:T(8,128)(2,1)}), bf16[8,96,128]{2,1,0:T(8,128)(2,1)S(1)}, u32[]{:S(2)}, u32[]{:S(2)}) async-start(bf16[8,96,128]{2,1,0:T(8,128)(2,1)} %copy.25), calls=%async_computation.1 | async-start | bytes 393216 | tf_op jit(solution)/shard_map/all_to_all | solution.py:119
  183.7 0.0 reduce-scatter.3.cloned.1.call-start
  183.7 5.9 %all-to-all-done.1 = bf16[8,96,128]{2,1,0:T(8,128)(2,1)S(1)} async-done(((bf16[8,96,128]{2,1,0:T(8,128)(2,1)}), bf16[8,96,128]{2,1,0:T(8,128)(2,1)S(1)}, u32[]{:S(2)}, u32[]{:S(2)}) %all-to-all-start.1) | async-done | bytes 196640 | tf_op jit(solution)/shard_map/all_to_all | solution.py:119
  189.6 3.2 %convert_reduce_fusion = f32[96,2048]{1,0:T(8,128)S(1)} fusion(bf16[8,128,2048]{2,1,0:T(8,128)(2,1)} %bitcast.43, bf16[8,96,128]{2,1,0:T(8,128)(2,1)S(1)} %all-to-all-done.1), kind=kOutput, calls=%fused_computation.8 | convolution fusion | flops 407175168 | bytes 5177344 | tf_op jit(solution)/shard_map/rgc,gcd->grd/dot_general | solution.py:123
  192.8 0.0 copy-done
  192.8 0.2 multiply_reduce_fusion
  193.0 0.0 copy-done.4
  193.0 0.1 multiply_convert_fusion.1
  193.2 0.4 stack.2
  193.6 41.6 %all_to_all.23 = bf16[8,96,2048]{2,1,0:T(8,128)(2,1)} all-to-all(bf16[8,96,2048]{2,1,0:T(8,128)(2,1)S(1)} %stack.2), channel_id=1, replica_groups=mesh['sp'=16,'tp_0'=4,'tp_1'=2] {'tp_0','tp_1'}, dimensions={0} | all-to-all | bytes 6291456 | tf_op jit(solution)/shard_map/all_to_all | solution.py:129
  235.1 5.1 %fusion.9 = f32[768,688]{0,1:T(8,128)S(1)} fusion(bf16[768,2048]{1,0:T(8,128)(2,1)} %bitcast.46, bf16[2048,2064]{0,1:T(8,128)(2,1)} %all-gather.8.cloned.1.call-done), kind=kOutput, calls=%fused_computation.14 | convolution fusion | flops 2164260864 | bytes 8077312 | tf_op jit(solution)/shard_map/dot_general | solution.py:132
  240.3 11.7 %convolution_convert_fusion = bf16[768,2048]{1,0:T(8,128)(2,1)} fusion(bf16[2048,2064]{0,1:T(8,128)(2,1)} %all-gather.8.cloned.1.call-done, f32[768,688]{0,1:T(8,128)S(1)} %fusion.9, bf16[768,2048]{1,0:T(8,128)(2,1)} %bitcast.47), kind=kOutput, calls=%fused_computation.9 | convolution fusion | flops 4333264896 | bytes 14041088 | tf_op jit(solution)/shard_map/dot_general | solution.py:135
  252.0 0.0 reduce-scatter.3.cloned.1.call-update
  252.0 0.0 reduce-scatter.5.cloned.1.call-start
  252.0 36.7 %reduce-scatter.3.cloned.1.call-done = bf16[192,2048]{1,0:T(8,128)(2,1)} async-done(((bf16[768,2048]{1,0:T(8,128)(2,1)}), bf16[192,2048]{1,0:T(8,128)(2,1)}) %reduce-scatter.3.cloned.1.call-update) | async-done | bytes 786448 | tf_op jit(solution)/shard_map/reduce_scatter | solution.py:54
  288.7 0.0 reduce-scatter.5.cloned.1.call-update
  288.7 13.3 %reduce-scatter.5.cloned.1.call-done = bf16[96,2048]{1,0:T(8,128)(2,1)} async-done(((bf16[192,2048]{1,0:T(8,128)(2,1)}), bf16[96,2048]{1,0:T(8,128)(2,1)}) %reduce-scatter.5.cloned.1.call-update) | async-done | bytes 393232 | tf_op jit(solution)/shard_map/reduce_scatter | solution.py:54
  302.0 1.9 add_convert_fusion
  (5 shorter events, 0.0 us)
Async XLA Ops:
  6.5 67.4 %all-gather.4.cloned.1.call-start = ((), (), s32[]{:S(2)}) async-start(), calls=%async_computation.5 | async-start | bytes 6684672 | tf_op jit(solution)/shard_map/all_gather | solution.py:49
  8.3 20.0 %copy-start.2 = (bf16[768,128]{1,0:T(8,128)(2,1)S(1)}, bf16[768,128]{1,0:T(8,128)(2,1)}, u32[]{:S(2)}) copy-start(bf16[768,128]{1,0:T(8,128)(2,1)} %param.11) | copy-start | bytes 589828
  8.4 175.4 %all-gather.6.cloned.1.call-start = ((), (), s32[]{:S(2)}) async-start(), calls=%async_computation.6 | async-start | bytes 4718592 | tf_op jit(solution)/shard_map/all_gather | solution.py:85
  10.5 72.4 %all-to-all-start = ((f32[16,768,2]{1,2,0:T(2,128)}), f32[16,768,2]{1,2,0:T(2,128)S(1)}, u32[]{:S(2)}, u32[]{:S(2)}) async-start(f32[16,768,2]{1,2,0:T(2,128)} %broadcast_in_dim.17), calls=%async_computation | async-start | bytes 196608 | tf_op jit(solution)/shard_map/all_to_all | solution.py:34
  18.9 216.2 %all-gather.8.cloned.1.call-start = ((), (), s32[]{:S(2)}) async-start(), calls=%async_computation.7 | async-start | bytes 8982528 | tf_op jit(solution)/shard_map/all_gather | solution.py:16
  78.2 4.7 %copy-start.3 = (f32[768,2]{0,1:T(2,128)S(1)}, f32[768,2]{0,1:T(2,128)}, u32[]{:S(2)}) copy-start(f32[768,2]{0,1:T(2,128)} %param.14) | copy-start | bytes 18436
  119.0 27.8 %copy-start.1 = (bf16[12288,128]{0,1:T(8,128)(2,1)S(1)}, bf16[12288,128]{0,1:T(8,128)(2,1)}, u32[]{:S(2)}) copy-start(bf16[12288,128]{0,1:T(8,128)(2,1)} %copy.23) | copy-start | bytes 9437188
  177.5 15.3 %copy-start = (bf16[96,2048]{1,0:T(8,128)(2,1)S(1)}, bf16[96,2048]{1,0:T(8,128)(2,1)}, u32[]{:S(2)}) copy-start(bf16[96,2048]{1,0:T(8,128)(2,1)} %param.10) | copy-start | bytes 1179652
  177.5 15.5 %copy-start.4 = (f32[2048]{0:T(1024)S(1)}, f32[2048]{0:T(1024)}, u32[]{:S(2)}) copy-start(f32[2048]{0:T(1024)} %param.16) | copy-start | bytes 24580
  178.7 10.9 %all-to-all-start.1 = ((bf16[8,96,128]{2,1,0:T(8,128)(2,1)}), bf16[8,96,128]{2,1,0:T(8,128)(2,1)S(1)}, u32[]{:S(2)}, u32[]{:S(2)}) async-start(bf16[8,96,128]{2,1,0:T(8,128)(2,1)} %copy.25), calls=%async_computation.1 | async-start | bytes 393216 | tf_op jit(solution)/shard_map/all_to_all | solution.py:119
  183.7 105.0 %reduce-scatter.3.cloned.1.call-start = ((), (), s32[]{:S(2)}) async-start(), calls=%async_computation.8 | async-start | bytes 3932160 | tf_op jit(solution)/shard_map/reduce_scatter | solution.py:54
  252.0 50.0 %reduce-scatter.5.cloned.1.call-start = ((), (), s32[]{:S(2)}) async-start(), calls=%async_computation.9 | async-start | bytes 1179648 | tf_op jit(solution)/shard_map/reduce_scatter | solution.py:54
Sparse Core Ops, SparseCore 0:
  9.5 64.4 all-gather.3
  75.7 32.1 all-gather.5
  110.0 75.6 all-gather.7
  252.1 36.5 reduce-scatter.2
  290.9 11.0 reduce-scatter.4
